TPU v7x, 32 devices: a whole 2x2x4 slice. The times are simulated.
32 devices in a mesh: rep: 2 (over x), fs: 8 (over z, y), tp: 2 (over core).
Axes of the slice: x: 2, y: 2, z: 4, core: 2. Of those that a mesh axis runs over, the one named last changes fastest.
Arguments:
- pre_gate: bfloat16 [12288, 4096], P(('rep', 'fs'), 'tp'), may hold values from -6 to 6
- pre_linear: bfloat16 [12288, 4096], P(('rep', 'fs'), 'tp'), may hold values from -6 to 6
- taps_gate: float32 [3, 4096], P(None, 'tp'), may hold values from -3.5 to 3.5
- taps_linear: float32 [3, 4096], P(None, 'tp'), may hold values from -3.5 to 3.5
- bias_gate: float32 [4096], P('tp'), may hold values from -3 to 3
- bias_linear: float32 [4096], P('tp'), may hold values from -3 to 3
- down_weight: bfloat16 [4096, 2048], P('tp', 'fs'), may hold values from -0.09375 to 0.09375
- out_grad: bfloat16 [12288, 2048], P(('rep', 'fs')), may hold values from -8 to 8
Outputs:
- grad_gate: bfloat16 [12288, 4096], P(('rep', 'fs'), 'tp')
- grad_linear: bfloat16 [12288, 4096], P(('rep', 'fs'), 'tp')
- grad_taps_gate: float32 [3, 4096], P(None, 'tp')
- grad_taps_linear: float32 [3, 4096], P(None, 'tp')
- grad_bias_gate: float32 [4096], P('tp')
- grad_bias_linear: float32 [4096], P('tp')
- grad_down: float32 [4096, 2048], P('tp', 'fs')
- row_norms: float32 [4096], P('tp')
All inputs are finite; a program needn't handle non-finite values.
Results may differ from a plain program's by a relative error of at most 0.0031.
Values may be sent and summed in bfloat16 or wider, within the bound.
No kernel may reach another device: no remote copies, remote signals or barrier semaphores. Data moves between devices by JAX's collectives and lax.ppermute only.
A program may use at most 128 MiB of HBM per device.

v0:
```python
import jax
import jax.numpy as jnp
from jax import lax
from jax.sharding import PartitionSpec as P


def convolve(values, taps, bias):
    length = values.shape[0]
    padded = jnp.pad(values, ((2, 0), (0, 0)))
    return (
        taps[0] * padded[0:length]
        + taps[1] * padded[1 : length + 1]
        + taps[2] * padded[2 : length + 2]
        + bias
    )


def convolve_back(grads, taps):
    length = grads.shape[0]
    padded = jnp.pad(grads, ((0, 2), (0, 0)))
    return (
        taps[0] * padded[2 : length + 2]
        + taps[1] * padded[1 : length + 1]
        + taps[2] * padded[0:length]
    )


def tap_grads(grads, values):
    length = values.shape[0]
    padded = jnp.pad(values, ((2, 0), (0, 0)))
    return jnp.stack([jnp.sum(grads * padded[j : j + length], axis=0) for j in range(3)])


def local(
    pre_gate, pre_linear, taps_gate, taps_linear, bias_gate, bias_linear, down_weight, out_grad
):
    gate_in = pre_gate.astype(jnp.float32)
    linear_in = pre_linear.astype(jnp.float32)
    gate_pre = convolve(gate_in, taps_gate, bias_gate)
    linear_pre = convolve(linear_in, taps_linear, bias_linear)
    sigma = jax.nn.sigmoid(gate_pre)
    silu_val = gate_pre * sigma
    hidden = (silu_val * linear_pre).astype(jnp.bfloat16)
    columns = out_grad
    grad_hidden = lax.dot_general(
        columns,
        lax.all_gather(down_weight, "fs", axis=1, tiled=True),
        (((1,), (1,)), ((), ())),
        preferred_element_type=jnp.float32,
    )
    grad_gate_pre = grad_hidden * linear_pre * sigma * (1.0 + gate_pre * (1.0 - sigma))
    grad_linear_pre = grad_hidden * silu_val
    grad_gate = convolve_back(grad_gate_pre, taps_gate).astype(jnp.bfloat16)
    grad_linear = convolve_back(grad_linear_pre, taps_linear).astype(jnp.bfloat16)
    conv_parts = (
        tap_grads(grad_gate_pre, gate_in),
        tap_grads(grad_linear_pre, linear_in),
        jnp.sum(grad_gate_pre, axis=0),
        jnp.sum(grad_linear_pre, axis=0),
    )
    grad_taps_gate, grad_taps_linear, grad_bias_gate, grad_bias_linear = lax.psum(
        (conv_parts[0], conv_parts[1], conv_parts[2], conv_parts[3]), ("rep", "fs")
    )
    columns = out_grad
    partial_grad = lax.psum_scatter(
        lax.dot_general(
            columns, hidden, (((0,), (0,)), ((), ())), preferred_element_type=jnp.float32
        ),
        "fs",
        scatter_dimension=0,
        tiled=True,
    )
    summed = lax.psum(partial_grad, "rep")
    grad_down = summed.T
    row_norms = lax.psum(jnp.sum(grad_down * grad_down, axis=1), "fs")
    return (
        grad_gate,
        grad_linear,
        grad_taps_gate,
        grad_taps_linear,
        grad_bias_gate,
        grad_bias_linear,
        grad_down,
        row_norms,
    )


def solution(mesh):
    in_specs = (
        P(("rep", "fs"), "tp"),
        P(("rep", "fs"), "tp"),
        P(None, "tp"),
        P(None, "tp"),
        P("tp"),
        P("tp"),
        P("tp", "fs"),
        P(("rep", "fs"), None),
    )
    out_specs = (
        P(("rep", "fs"), "tp"),
        P(("rep", "fs"), "tp"),
        P(None, "tp"),
        P(None, "tp"),
        P("tp"),
        P("tp"),
        P("tp", "fs"),
        P("tp"),
    )
    return jax.shard_map(local, mesh=mesh, in_specs=in_specs, out_specs=out_specs, check_vma=False)
```

profile of v0, /device:TPU:0, one launch (start us, length us, event | category | flops | bytes accessed | tf_op | source)
XLA Modules:
  0.0 668.1 jit_solution(7865275278848254621)
XLA Ops:
  7.2 0.0 all-gather.2.cloned.1.call-start
  7.2 0.7 all-gather.2.cloned.1.call-update
  7.9 0.0 reduce-scatter.2.cloned.1.call-start
  8.0 5.6 convert_element_type.24
  13.5 3.4 convert_element_type.23
  17.0 120.7 %all-gather.2.cloned.1.call-done = bf16[2048,2048]{1,0:T(8,128)(2,1)} async-done(((bf16[2048,256]{1,0:T(8,128)(2,1)}), bf16[2048,2048]{1,0:T(8,128)(2,1)}) %all-gather.2.cloned.1.call-update) | async-done | bytes 8388624 | tf_op jit(solution)/shard_map/all_gather | solution.py:47
  137.8 25.9 %fusion.4 = (f32[2048]{0:T(1024)}, f32[2048]{0:T(1024)S(1)}, f32[2048]{0:T(1024)S(1)}, f32[2048]{0:T(1024)S(1)}, f32[768,2048]{1,0:T(8,128)}, /*index=5*/f32[768,2048]{1,0:T(8,128)}, f32[768,2048]{1,0:T(8,128)}) fusion(bf16[768,2048]{1,0:T(8,128)(2,1)} %param.9, f32[768,2048]{1,0:T(8,128)} %convert_element_type.23, f32[2048]{0:T(1024)S(1)} %copy-done.7, ...), kind=kOutput, calls=%fused_computation.24 | convolution fusion | flops 6472327168 | bytes 46202880 | tf_op jit(solution)/shard_map/dot_general | solution.py:45
  163.7 19.0 %fusion.5 = (f32[2048]{0:T(1024)}, f32[2048]{0:T(1024)S(1)}, f32[2048]{0:T(1024)S(1)}, f32[2048]{0:T(1024)S(1)}, f32[768,2048]{1,0:T(8,128)}, /*index=5*/f32[768,2048]{1,0:T(8,128)}, bf16[768,2048]{1,0:T(8,128)(2,1)}) fusion(bf16[768,2048]{1,0:T(8,128)(2,1)} %param.8, f32[768,2048]{1,0:T(8,128)S(1)} %copy-done.1, f32[768,2048]{1,0:T(8,128)} %get-tuple-element.25, ...), kind=kLoop, calls=%fused_computation.25 | loop fusion | flops 45604864 | bytes 50397184 | tf_op jit(solution)/shard_map/reduce_sum | solution.py:58
  182.7 15.2 %convolution_bitcast_fusion = f32[2048,2048]{0,1:T(8,128)} fusion(bf16[768,2048]{1,0:T(8,128)(2,1)S(1)} %copy-done, f32[768,2048]{1,0:T(8,128)} %get-tuple-element.27, f32[768,2048]{1,0:T(8,128)} %get-tuple-element.25), kind=kOutput, calls=%fused_computation | convolution fusion | flops 6451888128 | bytes 32505856 | tf_op jit(solution)/shard_map/dot_general | solution.py:66
  197.8 0.0 reduce-scatter.2.cloned.1.call-update
  197.9 0.0 all-reduce.8.cloned.1.call-start
  197.9 278.5 %reduce-scatter.2.cloned.1.call-done = f32[256,2048]{0,1:T(8,128)} async-done(((f32[2048,2048]{0,1:T(8,128)}), f32[256,2048]{0,1:T(8,128)}) %reduce-scatter.2.cloned.1.call-update) | async-done | bytes 2097168 | tf_op jit(solution)/shard_map/reduce_scatter | solution.py:65
  476.5 0.0 all-reduce.10.cloned.1.call-start
  476.5 0.7 pad_maximum_fusion
  477.2 9.6 %add_convert_fusion.1 = bf16[768,2048]{1,0:T(8,128)(2,1)} fusion(f32[768,2048]{1,0:T(8,128)} %get-tuple-element.26, f32[2048]{0:T(1024)S(1)} %bitcast.28, f32[2048]{0:T(1024)S(1)} %bitcast.30, f32[2048]{0:T(1024)S(1)} %bitcast.26), kind=kLoop, calls=%fused_computation.9 | loop fusion | flops 9437184 | bytes 9461760 | tf_op jit(solution)/shard_map/convert_element_type | solution.py:53
  486.8 54.0 %all-reduce.8.cloned.1.call-done = f32[2048,256]{1,0:T(8,128)} async-done(((f32[2048,256]{1,0:T(8,128)}), f32[2048,256]{1,0:T(8,128)}) %all-reduce.8.cloned.1.call-update) | async-done | bytes 2097168 | tf_op jit(solution)/shard_map/psum | solution.py:73
  540.8 1.9 multiply_reduce_fusion.6
  542.8 22.3 %psum.47 = f32[2048]{0:T(1024)} all-reduce(f32[2048]{0:T(1024)S(1)} %multiply_reduce_fusion.6), channel_id=1, replica_groups=mesh['rep'=2,'fs'=8,'tp'=2] {'fs'}, use_global_device_ids=true, to_apply=%region_15.16 | all-reduce | flops 2048 | bytes 16384 | tf_op jit(solution)/shard_map/psum | solution.py:75
  565.1 88.1 %all-reduce.10.cloned.1.call-done = (f32[3,2048]{1,0:T(4,128)}, f32[3,2048]{1,0:T(4,128)}, f32[2048]{0:T(1024)}, f32[2048]{0:T(1024)}) async-done(((f32[3,2048]{1,0:T(4,128)}, f32[3,2048]{1,0:T(4,128)}, f32[2048]{0:T(1024)}, f32[2048]{0:T(1024)}), (f32[3,2048]{1,0:T(4,128)}, f32[3,2048]{1,0:T(4,128)}, f32[2048]{0:T(1024)}, f32[2048]{0:T(1024)})) %all-reduce.10.cloned.1.call-update) | async-done | bytes 65552 | tf_op jit(solution)/shard_map/psum | solution.py:61
  653.2 1.4 copy.21
  654.6 1.4 copy.22
  655.9 1.3 copy.23
  657.2 1.3 copy.24
  658.5 3.0 copy.25
  (20 shorter events, 0.1 us)
Async XLA Ops:
  7.2 130.6 %copy-start = (bf16[768,2048]{1,0:T(8,128)(2,1)S(1)}, bf16[768,2048]{1,0:T(8,128)(2,1)}, u32[]{:S(2)}) copy-start(bf16[768,2048]{1,0:T(8,128)(2,1)} %param.15) | copy-start | bytes 9437188
  7.2 130.5 %all-gather.2.cloned.1.call-start = ((), (), s32[]{:S(2)}) async-start(), calls=%async_computation.1 | async-start | bytes 9437184 | tf_op jit(solution)/shard_map/all_gather | solution.py:47
  7.9 468.5 %reduce-scatter.2.cloned.1.call-start = ((), (), s32[]{:S(2)}) async-start(), calls=%async_computation.2 | async-start | bytes 18874368 | tf_op jit(solution)/shard_map/reduce_scatter | solution.py:65
  8.0 5.6 copy-start.3
  13.5 3.4 copy-start.4
  13.5 3.5 copy-start.5
  13.5 124.2 %copy-start.7 = (f32[2048]{0:T(1024)S(1)}, f32[2048]{0:T(1024)}, u32[]{:S(2)}) copy-start(f32[2048]{0:T(1024)} %param.12) | copy-start | bytes 24580
  137.7 25.9 %copy-start.1 = (f32[768,2048]{1,0:T(8,128)S(1)}, f32[768,2048]{1,0:T(8,128)}, u32[]{:S(2)}) copy-start(f32[768,2048]{1,0:T(8,128)} %convert_element_type.24) | copy-start | bytes 18874372
  137.7 25.9 %copy-start.2 = (f32[768,2048]{1,0:T(8,128)S(1)}, f32[768,2048]{1,0:T(8,128)}, u32[]{:S(2)}) copy-start(f32[768,2048]{1,0:T(8,128)} %convert_element_type.23) | copy-start | bytes 18874372
  137.7 25.9 %copy-start.6 = (f32[2048]{0:T(1024)S(1)}, f32[2048]{0:T(1024)}, u32[]{:S(2)}) copy-start(f32[2048]{0:T(1024)} %param.13) | copy-start | bytes 24580
  197.9 343.0 %all-reduce.8.cloned.1.call-start = ((), (), s32[]{:S(2)}) async-start(), calls=%async_computation.3 | async-start | bytes 4194304 | tf_op jit(solution)/shard_map/psum | solution.py:73
  476.5 176.7 %all-reduce.10.cloned.1.call-start = ((), (), s32[]{:S(2)}) async-start(), calls=%async_computation.4 | async-start | bytes 163840 | tf_op jit(solution)/shard_map/psum | solution.py:61
Sparse Core Ops, SparseCore 0:
  10.0 127.6 all-gather.1
  198.0 278.3 reduce-scatter.1
  478.7 62.0 all-reduce.7
  547.2 105.9 all-reduce.9
where the time goes:
time: 669 us; the launch traced here: 668 us
  waiting for transfers between devices  542 us (81%)
  matrix products  41.1 us (6%)
  other arithmetic  40.2 us (6%)
  blocking collectives  22.3 us (3%)
  between operations  13.8 us (2%)
  local copies, waits for them, and re-layouts  8.47 us (1%)
    reduce_scatter x1, waiting for transfers between devices, local(): lax.psum_scatter(lax.dot_general(columns, hidden, (((0,), (0,)), ((), ())...  279 us
    all_gather x1, waiting for transfers between devices, local(): lax.all_gather(down_weight, 'fs', axis=1, tiled=True)  121 us
    psum x1, waiting for transfers between devices, local(): lax.psum((conv_parts[0], conv_parts[1], conv_parts[2], conv_parts[3]), ('...  88.1 us
    psum x1, waiting for transfers between devices, local(): summed = lax.psum(partial_grad, 'rep')  54 us
    dot_general x1, matrix products, local(): lax.dot_general(columns, lax.all_gather(down_weight, 'fs', axis=1, tiled=...  25.9 us
    psum x1, blocking collectives, local(): row_norms = lax.psum(jnp.sum(grad_down * grad_down, axis=1), 'fs')  22.3 us
    reduce_sum x1, other arithmetic, local(): jnp.sum(grad_gate_pre, axis=0)  19 us
    dot_general x1, matrix products, local(): lax.dot_general(columns, hidden, (((0,), (0,)), ((), ())), preferred_elem...  15.2 us
  transfers between devices with their start and end apart: 4, of which 4 were waited for; matrix products, arithmetic and copies ran while one was open for 3% of the time, Pallas kernels for 0%

commit v1 on v0

--- a/solution.py
+++ b/solution.py
@@ -59,7 +59,7 @@
         jnp.sum(grad_linear_pre, axis=0),
     )
     grad_taps_gate, grad_taps_linear, grad_bias_gate, grad_bias_linear = lax.psum(
-        (conv_parts[0], conv_parts[1], conv_parts[2], conv_parts[3]), ("rep", "fs")
+        lax.psum((conv_parts[0], conv_parts[1], conv_parts[2], conv_parts[3]), "fs"), "rep"
     )
     columns = out_grad
     partial_grad = lax.psum_scatter(

time: 669 us -> 656 us (0.981)
  blocking collectives: 22.3 us -> 0 us
  waiting for transfers between devices: 542 us -> 550 us
    psum x1 -> x0, blocking collectives: 22.3 us -> none  [local(): row_norms = lax.psum(jnp.sum(grad_down * grad_down, axis=1), 'fs')]
    psum x1, waiting for transfers between devices: 54 us -> 63.7 us  [local(): summed = lax.psum(partial_grad, 'rep')]
    psum x1 -> x2, waiting for transfers between devices: 88.1 us -> 86.4 us  [the longest x1 73.2 us: local(): lax.psum((conv_parts[0], conv_parts[1], conv_parts[2], conv_parts[3]), 'fs')]
  transfers between devices with their start and end apart: 4 -> 5, of which waited for: 4 -> 5; matrix products, arithmetic and copies ran while one was open for 3% -> 3% of each run, Pallas kernels for 0% -> 0%
where the time goes in v1:
time: 656 us; the launch traced here: 655 us
  waiting for transfers between devices  550 us (84%)
  matrix products  41.1 us (6%)
  other arithmetic  41 us (6%)
  between operations  13.9 us (2%)
  local copies, waits for them, and re-layouts  9.07 us (1%)
    reduce_scatter x1, waiting for transfers between devices, local(): lax.psum_scatter(lax.dot_general(columns, hidden, (((0,), (0,)), ((), ())...  279 us
    all_gather x1, waiting for transfers between devices, local(): lax.all_gather(down_weight, 'fs', axis=1, tiled=True)  121 us
    psum x1, waiting for transfers between devices, local(): lax.psum((conv_parts[0], conv_parts[1], conv_parts[2], conv_parts[3]), 'fs')  73.2 us
    psum x1, waiting for transfers between devices, local(): summed = lax.psum(partial_grad, 'rep')  63.7 us
    dot_general x1, matrix products, local(): lax.dot_general(columns, lax.all_gather(down_weight, 'fs', axis=1, tiled=...  25.9 us
    reduce_sum x1, other arithmetic, local(): jnp.sum(grad_gate_pre, axis=0)  19.5 us
    dot_general x1, matrix products, local(): lax.dot_general(columns, hidden, (((0,), (0,)), ((), ())), preferred_elem...  15.2 us
    psum x1, waiting for transfers between devices, local(): lax.psum(lax.psum((conv_parts[0], conv_parts[1], conv_parts[2], conv_part...  13.2 us
  transfers between devices with their start and end apart: 5, of which 5 were waited for; matrix products, arithmetic and copies ran while one was open for 3% of the time, Pallas kernels for 0%

profile of v1, /device:TPU:0, one launch (start us, length us, event | category | flops | bytes accessed | tf_op | source)
XLA Modules:
  0.0 655.3 jit_solution(3258698762246823246)
XLA Ops:
  7.2 0.7 all-gather.2.cloned.1.call-update
  7.9 0.0 reduce-scatter.2.cloned.1.call-start
  8.0 5.5 convert_element_type.24
  13.5 3.4 convert_element_type.23
  16.9 120.8 %all-gather.2.cloned.1.call-done = bf16[2048,2048]{1,0:T(8,128)(2,1)} async-done(((bf16[2048,256]{1,0:T(8,128)(2,1)}), bf16[2048,2048]{1,0:T(8,128)(2,1)}) %all-gather.2.cloned.1.call-update) | async-done | bytes 8388624 | tf_op jit(solution)/shard_map/all_gather | solution.py:47
  137.8 25.9 %fusion.4 = (f32[2048]{0:T(1024)}, f32[2048]{0:T(1024)S(1)}, f32[2048]{0:T(1024)S(1)}, f32[2048]{0:T(1024)S(1)}, f32[768,2048]{1,0:T(8,128)}, /*index=5*/f32[768,2048]{1,0:T(8,128)}, f32[768,2048]{1,0:T(8,128)}) fusion(bf16[768,2048]{1,0:T(8,128)(2,1)} %param.9, f32[768,2048]{1,0:T(8,128)} %convert_element_type.23, f32[2048]{0:T(1024)S(1)} %copy-done.8, ...), kind=kOutput, calls=%fused_computation.24 | convolution fusion | flops 6472327168 | bytes 46202880 | tf_op jit(solution)/shard_map/dot_general | solution.py:45
  163.7 19.5 %fusion.5 = (f32[2048]{0:T(1024)}, f32[2048]{0:T(1024)S(1)}, f32[2048]{0:T(1024)S(1)}, f32[2048]{0:T(1024)S(1)}, f32[768,2048]{1,0:T(8,128)}, /*index=5*/f32[768,2048]{1,0:T(8,128)}, bf16[768,2048]{1,0:T(8,128)(2,1)}) fusion(bf16[768,2048]{1,0:T(8,128)(2,1)} %param.8, f32[768,2048]{1,0:T(8,128)S(1)} %copy-done.1, f32[768,2048]{1,0:T(8,128)} %get-tuple-element.30, ...), kind=kLoop, calls=%fused_computation.25 | loop fusion | flops 45604864 | bytes 50397184 | tf_op jit(solution)/shard_map/reduce_sum | solution.py:58
  183.2 15.2 %convolution_bitcast_fusion = f32[2048,2048]{0,1:T(8,128)} fusion(bf16[768,2048]{1,0:T(8,128)(2,1)S(1)} %copy-done, f32[768,2048]{1,0:T(8,128)} %get-tuple-element.32, f32[768,2048]{1,0:T(8,128)} %get-tuple-element.30), kind=kOutput, calls=%fused_computation | convolution fusion | flops 6451888128 | bytes 32505856 | tf_op jit(solution)/shard_map/dot_general | solution.py:66
  198.4 0.0 all-reduce.10.cloned.1.call-start
  198.4 278.5 %reduce-scatter.2.cloned.1.call-done = f32[256,2048]{0,1:T(8,128)} async-done(((f32[2048,2048]{0,1:T(8,128)}), f32[256,2048]{0,1:T(8,128)}) %reduce-scatter.2.cloned.1.call-update) | async-done | bytes 2097168 | tf_op jit(solution)/shard_map/reduce_scatter | solution.py:65
  476.9 0.0 all-reduce.12.cloned.1.call-start
  477.0 0.7 pad_maximum_fusion
  477.7 63.7 %all-reduce.10.cloned.1.call-done = f32[2048,256]{1,0:T(8,128)} async-done(((f32[2048,256]{1,0:T(8,128)}), f32[2048,256]{1,0:T(8,128)}) %all-reduce.10.cloned.1.call-update) | async-done | bytes 2097168 | tf_op jit(solution)/shard_map/psum | solution.py:73
  541.3 2.5 multiply_reduce_fusion.6
  543.9 0.0 all-reduce.14.cloned.1.call-start
  543.9 73.2 %all-reduce.12.cloned.1.call-done = (f32[3,2048]{1,0:T(4,128)}, f32[3,2048]{1,0:T(4,128)}, f32[2048]{0:T(1024)}, f32[2048]{0:T(1024)}, f32[2048]{0:T(1024)}) async-done(((f32[3,2048]{1,0:T(4,128)}, f32[3,2048]{1,0:T(4,128)}, f32[2048]{0:T(1024)}, f32[2048]{0:T(1024)}, f32[2048]{0:T(1024)}), (f32[3,2048]{1,0:T(4,128)}, f32[3,2048]{1,0:T(4,128)}, f32[2048]{0:T(1024)}, f32[2048]{0:T(1024)}, ...) | async-done | bytes 73744 | tf_op jit(solution)/shard_map/psum | solution.py:62
  617.1 9.4 %add_convert_fusion.1 = bf16[768,2048]{1,0:T(8,128)(2,1)} fusion(f32[768,2048]{1,0:T(8,128)} %get-tuple-element.31, f32[2048]{0:T(1024)S(1)} %bitcast.28, f32[2048]{0:T(1024)S(1)} %bitcast.30, f32[2048]{0:T(1024)S(1)} %bitcast.26), kind=kLoop, calls=%fused_computation.9 | loop fusion | flops 9437184 | bytes 9461760 | tf_op jit(solution)/shard_map/convert_element_type | solution.py:53
  626.6 13.2 %all-reduce.14.cloned.1.call-done = (f32[3,2048]{1,0:T(4,128)}, f32[3,2048]{1,0:T(4,128)}, f32[2048]{0:T(1024)}, f32[2048]{0:T(1024)}) async-done(((f32[3,2048]{1,0:T(4,128)}, f32[3,2048]{1,0:T(4,128)}, f32[2048]{0:T(1024)}, f32[2048]{0:T(1024)}), (f32[3,2048]{1,0:T(4,128)}, f32[3,2048]{1,0:T(4,128)}, f32[2048]{0:T(1024)}, f32[2048]{0:T(1024)})) %all-reduce.14.cloned.1.call-update) | async-done | bytes 65552 | tf_op jit(solution)/shard_map/psum | solution.py:61
  639.8 1.4 copy.26
  641.1 1.4 copy.27
  642.5 1.3 copy.28
  643.8 1.3 copy.29
  645.1 3.0 copy.30
  648.2 0.6 copy.31
  (25 shorter events, 0.2 us)
Async XLA Ops:
  7.2 130.6 %copy-start = (bf16[768,2048]{1,0:T(8,128)(2,1)S(1)}, bf16[768,2048]{1,0:T(8,128)(2,1)}, u32[]{:S(2)}) copy-start(bf16[768,2048]{1,0:T(8,128)(2,1)} %param.15) | copy-start | bytes 9437188
  7.2 130.5 %all-gather.2.cloned.1.call-start = ((), (), s32[]{:S(2)}) async-start(), calls=%async_computation.1 | async-start | bytes 9437184 | tf_op jit(solution)/shard_map/all_gather | solution.py:47
  7.9 469.0 %reduce-scatter.2.cloned.1.call-start = ((), (), s32[]{:S(2)}) async-start(), calls=%async_computation.2 | async-start | bytes 18874368 | tf_op jit(solution)/shard_map/reduce_scatter | solution.py:65
  8.0 5.5 copy-start.3
  13.4 3.4 copy-start.4
  13.4 3.5 copy-start.5
  13.4 124.3 %copy-start.8 = (f32[2048]{0:T(1024)S(1)}, f32[2048]{0:T(1024)}, u32[]{:S(2)}) copy-start(f32[2048]{0:T(1024)} %param.12) | copy-start | bytes 24580
  137.7 25.9 %copy-start.1 = (f32[768,2048]{1,0:T(8,128)S(1)}, f32[768,2048]{1,0:T(8,128)}, u32[]{:S(2)}) copy-start(f32[768,2048]{1,0:T(8,128)} %convert_element_type.24) | copy-start | bytes 18874372
  137.7 25.9 %copy-start.2 = (f32[768,2048]{1,0:T(8,128)S(1)}, f32[768,2048]{1,0:T(8,128)}, u32[]{:S(2)}) copy-start(f32[768,2048]{1,0:T(8,128)} %convert_element_type.23) | copy-start | bytes 18874372
  137.7 25.9 %copy-start.6 = (f32[2048]{0:T(1024)S(1)}, f32[2048]{0:T(1024)}, u32[]{:S(2)}) copy-start(f32[2048]{0:T(1024)} %param.13) | copy-start | bytes 24580
  198.4 343.0 %all-reduce.10.cloned.1.call-start = ((), (), s32[]{:S(2)}) async-start(), calls=%async_computation.3 | async-start | bytes 4194304 | tf_op jit(solution)/shard_map/psum | solution.py:73
  476.9 140.2 %all-reduce.12.cloned.1.call-start = ((), (), s32[]{:S(2)}) async-start(), calls=%async_computation.4 | async-start | bytes 180224 | tf_op jit(solution)/shard_map/psum | solution.py:62
  543.9 95.9 %all-reduce.14.cloned.1.call-start = ((), (), s32[]{:S(2)}) async-start(), calls=%async_computation.5 | async-start | bytes 163840 | tf_op jit(solution)/shard_map/psum | solution.py:61
  617.1 31.0 %copy-start.7 = (f32[2048]{0:T(1024)S(1)}, f32[2048]{0:T(1024)}, u32[]{:S(2)}) copy-start(f32[2048]{0:T(1024)} %get-tuple-element.50) | copy-start | bytes 24580
Sparse Core Ops, SparseCore 0:
  10.0 127.6 all-gather.1
  198.5 278.3 reduce-scatter.1
  479.2 62.0 all-reduce.9
  545.7 71.4 all-reduce.11
  619.4 20.3 all-reduce.13
